TPU v7x, 256 devices: a whole 4x4x8 slice. The times are simulated.
256 devices in a mesh: ep: 32 (over z, x), tp: 8 (over y, core).
Axes of the slice: x: 4, y: 4, z: 8, core: 2. Of those that a mesh axis runs over, the one named last changes fastest.
Arguments:
- resid: bfloat16 [1024, 2048], P('ep'), may hold values from -6 to 6
- norm_gain: bfloat16 [2048], replicated, may hold values from 0.099609375 to 1.8984375
- w_query: bfloat16 [2048, 1024], P(None, 'tp'), may hold values from -0.125 to 0.125
- w_key: bfloat16 [2048, 1024], P(None, 'tp'), may hold values from -0.125 to 0.125
- w_value: bfloat16 [2048, 1024], P(None, 'tp'), may hold values from -0.125 to 0.125
- w_gate: bfloat16 [2048, 1024], P(None, 'tp'), may hold values from -0.125 to 0.125
- head_gain: bfloat16 [1024], P('tp'), may hold values from 0.099609375 to 1.8984375
- w_output: bfloat16 [1024, 2048], P('tp'), may hold values from -0.1875 to 0.1875
- state: float32 [1024, 8, 128, 128], P('ep', 'tp'), may hold values from -0.6 to 0.6
- positions: int32 [1024], P('ep'), may hold values from 1024 to 8191
- ffn_gain: bfloat16 [2048], replicated, may hold values from 0.099609375 to 1.8984375
- w_mix: bfloat16 [2048], replicated, may hold values from -0.125 to 0.125
- dense_gate: bfloat16 [2048, 5632], P('tp', 'ep'), may hold values from -0.125 to 0.125
- dense_up: bfloat16 [2048, 5632], P('tp', 'ep'), may hold values from -0.125 to 0.125
- dense_down: bfloat16 [5632, 2048], P('ep', 'tp'), may hold values from -0.15625 to 0.15625
- routes: int32 [1024, 2], P('ep'), may hold values from 0 to 31, all different within a row; in each aligned block of 32 rows (0 to 31, 32 to 63, ...) at most 4 rows name the same one
- route_weight: bfloat16 [1024, 2], P('ep'), may hold values from 0.19921875 to 1
- expert_gate: bfloat16 [32, 2048, 4096], P('ep', None, 'tp'), may hold values from -0.125 to 0.125
- expert_up: bfloat16 [32, 2048, 4096], P('ep', None, 'tp'), may hold values from -0.125 to 0.125
- expert_down: bfloat16 [32, 4096, 2048], P('ep', 'tp'), may hold values from -0.09375 to 0.09375
Outputs:
- final: bfloat16 [1024, 2048], P('ep', 'tp')
- new_state: float32 [1024, 8, 128, 128], P('ep', 'tp')
Inputs may be any that keep to these rules, and one draw needn't show every extreme that they name: `routes`: each row names 2 different experts; in the rows of one index of ep no expert is named by more than 4 rows, a bound that some block reaches; every expert is named by some row.
All inputs are finite; a program needn't handle non-finite values.
Results may differ from a plain program's by a relative error of at most 0.018.
Values may be sent and summed in bfloat16 or wider, within the bound.
No kernel may reach another device: no remote copies, remote signals or barrier semaphores. Data moves between devices by JAX's collectives and lax.ppermute only.
A program may use at most 64 MiB of HBM per device.

v0:
```python
import jax
import jax.numpy as jnp
from jax import lax
from jax.sharding import PartitionSpec as P

EPSILON = 1e-06
THETA = 10000.0


def split_up(value, dim, length):
    before, after = (value.shape[:dim], value.shape[dim + 1 :])
    return jnp.moveaxis(value.reshape(*before, length, -1, *after), dim, 0)


def sent_and_summed(value, axis, dim):
    tiles = split_up(value, dim, lax.axis_size(axis))
    arrived = lax.all_to_all(tiles, axis, split_axis=0, concat_axis=0, tiled=True)
    return arrived.astype(jnp.float32).sum(axis=0)


def copy_for_each(value, axis):
    copies = jnp.broadcast_to(value, (lax.axis_size(axis), *value.shape))
    return lax.all_to_all(copies, axis, split_axis=0, concat_axis=0, tiled=True)


def of_everyone(value, axis):
    everything = copy_for_each(value, axis)
    return jnp.sum(everything.astype(jnp.float32), axis=0)


def in_order(tiles, dim):
    dims = list(tiles.shape[1:])
    dims[dim] *= tiles.shape[0]
    return jnp.moveaxis(tiles, 0, dim).reshape(dims)


def gather_directly(value, axis, dim):
    tiles = copy_for_each(value, axis)
    return in_order(tiles, dim)


def packed_total(arrays, axis):
    flat, at, outs = (jnp.concatenate([a.reshape(-1) for a in arrays]), 0, [])
    running = lax.psum(flat, axis)
    for a in arrays:
        outs.append(running[at : at + a.size].reshape(a.shape))
        at += a.size
    return tuple(outs)


def rms_norm(inputs, scaling):
    square = jnp.mean(inputs * inputs, axis=-1, keepdims=True)
    return inputs * lax.rsqrt(square + EPSILON) * scaling.astype(jnp.float32)


def rotate(inputs, places):
    halfway = inputs.shape[-1] // 2
    inverse = THETA ** (-jnp.arange(halfway, dtype=jnp.float32) / halfway)
    angles = places.astype(jnp.float32)[:, None] * inverse[None, :]
    cosine = jnp.cos(angles)[:, None, :]
    sine_of = jnp.sin(angles)[:, None, :]
    former = inputs[..., :halfway]
    latter = inputs[..., halfway:]
    return jnp.concatenate(
        [former * cosine - latter * sine_of, former * sine_of + latter * cosine], axis=-1
    )


def retain(queries, keys_in, values_in, gating, memory, places, head_first, head_gain):
    seqs_here = queries.shape[0]
    heads_here = memory.shape[1]
    head_size = memory.shape[2]
    head_shape = (seqs_here, heads_here, head_size)
    query_rot = rotate(queries.astype(jnp.float32).reshape(head_shape), places)
    key_rot = rotate(keys_in.astype(jnp.float32).reshape(head_shape), places) * head_size ** (-0.5)
    value_heads = values_in.astype(jnp.float32).reshape(head_shape)
    head_index = head_first + jnp.arange(heads_here, dtype=jnp.float32)
    decays = 1.0 - jnp.exp2(-1.0 - 1.5 * head_index)
    within = jnp.sum(query_rot * key_rot, axis=-1, keepdims=True) * value_heads
    carried = jnp.einsum("shd,shde->she", query_rot, memory) * decays[None, :, None]
    mixture = within + carried
    new_memory = (
        decays[None, :, None, None] * memory + key_rot[:, :, :, None] * value_heads[:, :, None, :]
    )
    centre = jnp.mean(mixture, axis=-1, keepdims=True)
    spread = jnp.mean(jnp.square(mixture - centre), axis=-1, keepdims=True)
    normed = ((mixture - centre) * lax.rsqrt(spread + EPSILON)).reshape(
        seqs_here, heads_here * head_size
    )
    normed = normed * head_gain.astype(jnp.float32)
    output = (jax.nn.silu(gating.astype(jnp.float32)) * normed).astype(jnp.bfloat16)
    return (output, new_memory)


def expert_hidden(chosen, gate_weight, up_weight):
    gate_value = jnp.dot(chosen, gate_weight, preferred_element_type=jnp.float32)
    up_value = jnp.dot(chosen, up_weight, preferred_element_type=jnp.float32)
    return (jax.nn.silu(gate_value) * up_value).astype(jnp.bfloat16)


def padded_experts(
    normed_mid, routes, route_weight, expert_gate, expert_up, expert_down, capacity, experts_all
):
    seq_dev, model_width = normed_mid.shape
    top_count = routes.shape[1]
    flat_ids = routes.reshape(-1)
    expert_ids = jnp.arange(experts_all, dtype=jnp.int32)
    onehot = (flat_ids[:, None] == expert_ids[None, :]).astype(jnp.int32)
    ranks = jnp.sum((jnp.cumsum(onehot, axis=0) - 1) * onehot, axis=1)
    slot_ids = flat_ids * capacity + ranks
    slot_range = jnp.arange(experts_all * capacity, dtype=jnp.int32)
    dispatch = (slot_range[:, None] == slot_ids[None, :]).astype(jnp.bfloat16)
    repeated = jnp.repeat(normed_mid, top_count, axis=0)
    outgoing = jnp.dot(dispatch, repeated, preferred_element_type=jnp.float32).astype(jnp.bfloat16)
    outgoing = outgoing.reshape(experts_all, capacity, model_width)
    arrived = lax.all_to_all(outgoing, "ep", split_axis=0, concat_axis=0, tiled=True)
    sources = arrived.shape[0]
    items = arrived.shape[1]
    hidden_e = expert_hidden(
        arrived.reshape(sources * items, model_width), expert_gate[0], expert_up[0]
    )
    partial_value = jnp.dot(hidden_e, expert_down[0], preferred_element_type=jnp.float32)
    summed = sent_and_summed(partial_value.astype(jnp.bfloat16), "tp", 1).astype(jnp.bfloat16)
    returned = lax.all_to_all(
        summed.reshape(sources, items, summed.shape[1]),
        "ep",
        split_axis=0,
        concat_axis=0,
        tiled=True,
    )
    flat_back = returned.reshape(experts_all * capacity, returned.shape[2])
    weighted = flat_back[slot_ids].astype(jnp.float32) * route_weight.reshape(-1)[:, None].astype(
        jnp.float32
    )
    return jnp.sum(weighted.reshape(seq_dev, top_count, weighted.shape[1]), axis=1)


def per_device(
    resid,
    norm_gain,
    w_query,
    w_key,
    w_value,
    w_gate,
    head_gain,
    w_output,
    state,
    positions,
    ffn_gain,
    w_mix,
    dense_gate,
    dense_up,
    dense_down,
    routes,
    route_weight,
    expert_gate,
    expert_up,
    expert_down,
):
    seq_dev = resid.shape[0]
    model_width = resid.shape[1]
    tp_count = lax.axis_size("tp")
    ep_count = lax.axis_size("ep")
    model_tp = model_width // tp_count
    tp_index = lax.axis_index("tp")
    normed_in = rms_norm(resid.astype(jnp.float32), norm_gain).astype(jnp.bfloat16)

    def project(weight):
        return jnp.dot(normed_in, weight, preferred_element_type=jnp.float32).astype(jnp.bfloat16)

    heads_here = state.shape[1]
    head_first = (tp_index * heads_here).astype(jnp.float32)
    retained, new_state = retain(
        project(w_query),
        project(w_key),
        project(w_value),
        project(w_gate),
        state,
        positions,
        head_first,
        head_gain,
    )
    partial_value = jnp.dot(retained, w_output, preferred_element_type=jnp.float32)
    attention = of_everyone(partial_value.astype(jnp.bfloat16), "tp").astype(jnp.float32)
    middle = resid.astype(jnp.float32) + attention
    normed_mid = rms_norm(middle, ffn_gain).astype(jnp.bfloat16)
    mixing = jax.nn.sigmoid(jnp.dot(normed_mid, w_mix[:, None], preferred_element_type=jnp.float32))

    def own_columns(matrix):
        return lax.dynamic_slice_in_dim(matrix, tp_index * model_tp, model_tp, 1)

    top_count = routes.shape[1]
    capacity = max(2, 2 * seq_dev * top_count // ep_count)
    dense_rows = gather_directly(own_columns(normed_mid), "ep", 0)
    moe_out = padded_experts(
        normed_mid, routes, route_weight, expert_gate, expert_up, expert_down, capacity, ep_count
    )
    gate_part = jnp.dot(dense_rows, dense_gate, preferred_element_type=jnp.float32)
    up_part = jnp.dot(dense_rows, dense_up, preferred_element_type=jnp.float32)
    gate_sum, up_sum = tuple(
        (
            part.astype(jnp.float32)
            for part in packed_total(
                (gate_part.astype(jnp.bfloat16), up_part.astype(jnp.bfloat16)), "tp"
            )
        )
    )
    dense_hidden = (jax.nn.silu(gate_sum) * up_sum).astype(jnp.bfloat16)
    dense_out = sent_and_summed(
        jnp.dot(dense_hidden, dense_down, preferred_element_type=jnp.float32).astype(jnp.bfloat16),
        "ep",
        0,
    )
    final = (own_columns(middle) + moe_out + mixing * dense_out).astype(jnp.bfloat16)
    return (final, new_state)


def solution(mesh):
    in_specs = (
        P("ep", None),
        P(),
        P(None, "tp"),
        P(None, "tp"),
        P(None, "tp"),
        P(None, "tp"),
        P("tp"),
        P("tp", None),
        P("ep", "tp", None, None),
        P("ep"),
        P(),
        P(),
        P("tp", "ep"),
        P("tp", "ep"),
        P("ep", "tp"),
        P("ep", None),
        P("ep", None),
        P("ep", None, "tp"),
        P("ep", None, "tp"),
        P("ep", "tp", None),
    )
    out_specs = (P("ep", "tp"), P("ep", "tp", None, None))
    return jax.shard_map(
        per_device, mesh=mesh, in_specs=in_specs, out_specs=out_specs, check_vma=False
    )
```

profile of v0, /device:TPU:24, one launch (start us, length us, event | category | flops | bytes accessed | tf_op | source)
XLA Modules:
  0.0 206.2 jit_solution(7254978397219586404)
XLA Ops:
  8.7 1.0 fusion.25
  10.5 1.4 fusion.18
  11.9 1.4 fusion.20
  13.6 2.0 fusion.66
  16.8 1.5 convolution_convert_fusion.2
  18.4 1.1 broadcast_in_dim.6
  19.5 5.4 %all-to-all-start = ((bf16[8,32,2048]{2,1,0:T(8,128)(2,1)}), bf16[8,32,2048]{2,1,0:T(8,128)(2,1)S(1)}, u32[]{:S(2)}, u32[]{:S(2)}) async-start(bf16[8,32,2048]{2,1,0:T(8,128)(2,1)} %broadcast_in_dim.6), calls=%async_computation | async-start | bytes 2097152 | tf_op jit(solution)/shard_map/all_to_all | solution.py:23
  25.0 13.7 %all-to-all-done = bf16[8,32,2048]{2,1,0:T(8,128)(2,1)S(1)} async-done(((bf16[8,32,2048]{2,1,0:T(8,128)(2,1)}), bf16[8,32,2048]{2,1,0:T(8,128)(2,1)S(1)}, u32[]{:S(2)}, u32[]{:S(2)}) %all-to-all-start) | async-done | bytes 1048608 | tf_op jit(solution)/shard_map/all_to_all | solution.py:23
  40.7 10.6 %all-to-all-start.4 = ((bf16[32,32,256]{2,1,0:T(8,128)(2,1)}), bf16[32,32,256]{2,1,0:T(8,128)(2,1)S(1)}, u32[]{:S(2)}, u32[]{:S(2)}) async-start(bf16[32,32,256]{2,1,0:T(8,128)(2,1)} %broadcast_in_dim.8), calls=%async_computation.4 | async-start | bytes 1048576 | tf_op jit(solution)/shard_map/all_to_all | solution.py:23
  54.7 14.1 %all-to-all-done.4 = bf16[32,32,256]{2,1,0:T(8,128)(2,1)S(1)} async-done(((bf16[32,32,256]{2,1,0:T(8,128)(2,1)}), bf16[32,32,256]{2,1,0:T(8,128)(2,1)S(1)}, u32[]{:S(2)}, u32[]{:S(2)}) %all-to-all-start.4) | async-done | bytes 524320 | tf_op jit(solution)/shard_map/all_to_all | solution.py:23
  68.8 4.7 %all-to-all-start.1 = ((bf16[32,4,2048]{2,1,0:T(4,128)(2,1)}), bf16[32,4,2048]{2,1,0:T(4,128)(2,1)S(1)}, u32[]{:S(2)}, u32[]{:S(2)}) async-start(bf16[32,4,2048]{2,1,0:T(4,128)(2,1)} %reshape.385), calls=%async_computation.1 | async-start | bytes 1048576 | tf_op jit(solution)/shard_map/all_to_all | solution.py:116
  73.5 1.2 convolution_convert_fusion.4
  74.7 2.0 convolution_convert_fusion.5
  76.7 1.2 copy.40
  77.9 1.4 reshape.391
  80.2 1.9 pad_maximum_fusion
  82.1 8.3 %all-to-all-done.1 = bf16[32,4,2048]{2,1,0:T(4,128)(2,1)S(1)} async-done(((bf16[32,4,2048]{2,1,0:T(4,128)(2,1)}), bf16[32,4,2048]{2,1,0:T(4,128)(2,1)S(1)}, u32[]{:S(2)}, u32[]{:S(2)}) %all-to-all-start.1) | async-done | bytes 524320 | tf_op jit(solution)/shard_map/all_to_all | solution.py:116
  90.6 2.0 fusion.3
  92.6 2.5 %convolution_convert_fusion = bf16[128,2048]{1,0:T(8,128)(2,1)S(1)} fusion(bf16[1,512,2048]{2,1,0:T(8,128)(2,1)S(1)} %copy-done, bf16[128,2048]{1,0:T(8,128)(2,1)S(1)} %reshape.386, bf16[1,2048,512]{2,1,0:T(8,128)(2,1)} %param.38, f32[128,512]{1,0:T(8,128)S(1)} %fusion.3), kind=kOutput, calls=%fused_computation.1 | convolution fusion | flops 537526272 | bytes 5505024 | tf_op jit(solution)/shard_map/dot_general | solution.py:122
  95.9 6.1 %all-to-all-start.2 = ((bf16[8,128,256]{2,1,0:T(8,128)(2,1)}), bf16[8,128,256]{2,1,0:T(8,128)(2,1)}, u32[]{:S(2)}, u32[]{:S(2)}) async-start(bf16[8,128,256]{2,1,0:T(8,128)(2,1)} %bitcast.85), calls=%async_computation.2 | async-start | bytes 1048576 | tf_op jit(solution)/shard_map/all_to_all | solution.py:17
  102.0 47.7 %all-reduce.2.cloned.1.call-done = bf16[360448]{0:T(1024)(128)(2,1)} async-done(((bf16[360448]{0:T(1024)(128)(2,1)}), bf16[360448]{0:T(1024)(128)(2,1)}) %all-reduce.2.cloned.1.call-update) | async-done | bytes 720912 | tf_op jit(solution)/shard_map/psum | solution.py:44
  149.8 1.2 slice_convert_fusion.1
  150.9 1.7 reshape.401
  152.7 1.7 reshape.402
  154.4 1.1 reduce_sum.102
  156.1 9.8 %all-to-all-start.3 = ((bf16[32,4,256]{2,1,0:T(4,128)(2,1)}), bf16[32,4,256]{2,1,0:T(4,128)(2,1)S(1)}, u32[]{:S(2)}, u32[]{:S(2)}) async-start(bf16[32,4,256]{2,1,0:T(4,128)(2,1)} %reshape.388), calls=%async_computation.3 | async-start | bytes 131072 | tf_op jit(solution)/shard_map/all_to_all | solution.py:124
  166.0 2.8 %convolution_convert_fusion.3 = bf16[1024,256]{1,0:T(8,128)(2,1)} fusion(bf16[176,256]{1,0:T(8,128)(2,1)S(1)} %copy-done.17, f32[1024,176]{1,0:T(8,128)} %reshape.402, f32[1024,176]{1,0:T(8,128)} %reshape.401), kind=kOutput, calls=%fused_computation.13 | convolution fusion | flops 93618176 | bytes 2056192 | tf_op jit(solution)/shard_map/dot_general | solution.py:210
  168.8 7.4 %all-to-all-done.3 = bf16[32,4,256]{2,1,0:T(4,128)(2,1)S(1)} async-done(((bf16[32,4,256]{2,1,0:T(4,128)(2,1)}), bf16[32,4,256]{2,1,0:T(4,128)(2,1)S(1)}, u32[]{:S(2)}, u32[]{:S(2)}) %all-to-all-start.3) | async-done | bytes 65568 | tf_op jit(solution)/shard_map/all_to_all | solution.py:124
  176.2 3.9 %all-to-all-start.5 = ((bf16[32,32,256]{2,1,0:T(8,128)(2,1)}), bf16[32,32,256]{2,1,0:T(8,128)(2,1)S(1)}, u32[]{:S(2)}, u32[]{:S(2)}) async-start(bf16[32,32,256]{2,1,0:T(8,128)(2,1)} %bitcast.18), calls=%async_computation.5 | async-start | bytes 1048576 | tf_op jit(solution)/shard_map/all_to_all | solution.py:17
  180.4 2.9 %multiply_add_fusion = f32[32,1,128,128]{3,2,1,0:T(8,128)} fusion(f32[32,1,128,128]{3,2,1,0:T(8,128)} %param.28, f32[32,128]{1,0:T(8,128)S(1)} %copy-done.9, f32[32,128]{1,0:T(8,128)S(1)} %maximum_multiply_fusion.1, f32[]{:T(128)S(6)} %sub.37), kind=kLoop, calls=%fused_computation.11 | loop fusion | flops 1572864 | bytes 4227076 | tf_op jit(solution)/shard_map/add | solution.py:83
  184.4 13.4 %all-to-all-done.5 = bf16[32,32,256]{2,1,0:T(8,128)(2,1)S(1)} async-done(((bf16[32,32,256]{2,1,0:T(8,128)(2,1)}), bf16[32,32,256]{2,1,0:T(8,128)(2,1)S(1)}, u32[]{:S(2)}, u32[]{:S(2)}) %all-to-all-start.5) | async-done | bytes 524320 | tf_op jit(solution)/shard_map/all_to_all | solution.py:17
  197.9 1.4 add_convert_fusion
  (86 shorter events, 13.0 us)
Async XLA Ops:
  7.2 85.5 %copy-start = (bf16[1,512,2048]{2,1,0:T(8,128)(2,1)S(1)}, bf16[1,512,2048]{2,1,0:T(8,128)(2,1)}, u32[]{:S(2)}) copy-start(bf16[1,512,2048]{2,1,0:T(8,128)(2,1)} %param.39) | copy-start | bytes 6291460
  7.2 8.4 %copy-start.1 = (bf16[32,2048]{1,0:T(8,128)(2,1)S(1)}, bf16[32,2048]{1,0:T(8,128)(2,1)}, u32[]{:S(2)}) copy-start(bf16[32,2048]{1,0:T(8,128)(2,1)} %param.20) | copy-start | bytes 393220
  7.2 8.4 %copy-start.5 = (bf16[2048,128]{1,0:T(8,128)(2,1)S(1)}, bf16[2048,128]{1,0:T(8,128)(2,1)}, u32[]{:S(2)}) copy-start(bf16[2048,128]{1,0:T(8,128)(2,1)} %param.24) | copy-start | bytes 1572868
  10.5 6.3 %copy-start.6 = (bf16[128,2048]{1,0:T(8,128)(2,1)S(1)}, bf16[128,2048]{1,0:T(8,128)(2,1)}, u32[]{:S(2)}) copy-start(bf16[128,2048]{1,0:T(8,128)(2,1)} %param.27) | copy-start | bytes 1572868
  13.4 4.9 %copy-start.7 = (f32[32,1,64]{2,0,1:T(8,128)}, f32[32,1,64]{2,0,1:T(8,128)S(1)}, u32[]{:S(2)}) copy-start(f32[32,1,64]{2,0,1:T(8,128)S(1)} %get-tuple-element.15) | copy-start | bytes 24580
  16.8 8.1 %copy-start.10 = (bf16[2048]{0:T(1024)(128)(2,1)S(1)}, bf16[2048]{0:T(1024)(128)(2,1)}, u32[]{:S(2)}) copy-start(bf16[2048]{0:T(1024)(128)(2,1)} %param.30) | copy-start | bytes 12292
  16.8 8.1 %copy-start.12 = (s32[32,2]{0,1:T(2,128)S(1)}, s32[32,2]{0,1:T(2,128)}, u32[]{:S(2)}) copy-start(s32[32,2]{0,1:T(2,128)} %param.35) | copy-start | bytes 772
  19.5 19.3 %all-to-all-start = ((bf16[8,32,2048]{2,1,0:T(8,128)(2,1)}), bf16[8,32,2048]{2,1,0:T(8,128)(2,1)S(1)}, u32[]{:S(2)}, u32[]{:S(2)}) async-start(bf16[8,32,2048]{2,1,0:T(8,128)(2,1)} %broadcast_in_dim.6), calls=%async_computation | async-start | bytes 2097152 | tf_op jit(solution)/shard_map/all_to_all | solution.py:23
  39.0 0.7 copy-start.2
  39.9 13.4 %copy-start.3 = (bf16[32,2048]{1,0:T(8,128)(2,1)}, bf16[32,2048]{1,0:T(8,128)(2,1)S(1)}, u32[]{:S(2)}) copy-start(bf16[32,2048]{1,0:T(8,128)(2,1)S(1)} %multiply_convert_fusion.2) | copy-start | bytes 393220
  40.7 28.1 %all-to-all-start.4 = ((bf16[32,32,256]{2,1,0:T(8,128)(2,1)}), bf16[32,32,256]{2,1,0:T(8,128)(2,1)S(1)}, u32[]{:S(2)}, u32[]{:S(2)}) async-start(bf16[32,32,256]{2,1,0:T(8,128)(2,1)} %broadcast_in_dim.8), calls=%async_computation.4 | async-start | bytes 1048576 | tf_op jit(solution)/shard_map/all_to_all | solution.py:23
  52.6 0.5 copy-start.13
  68.8 21.7 %all-to-all-start.1 = ((bf16[32,4,2048]{2,1,0:T(4,128)(2,1)}), bf16[32,4,2048]{2,1,0:T(4,128)(2,1)S(1)}, u32[]{:S(2)}, u32[]{:S(2)}) async-start(bf16[32,4,2048]{2,1,0:T(4,128)(2,1)} %reshape.385), calls=%async_computation.1 | async-start | bytes 1048576 | tf_op jit(solution)/shard_map/all_to_all | solution.py:116
  73.5 76.3 %all-reduce.2.cloned.1.call-start = ((), (), s32[]{:S(2)}) async-start(), calls=%async_computation.6 | async-start | bytes 1441792 | tf_op jit(solution)/shard_map/psum | solution.py:44
  95.9 58.4 %all-to-all-start.2 = ((bf16[8,128,256]{2,1,0:T(8,128)(2,1)}), bf16[8,128,256]{2,1,0:T(8,128)(2,1)}, u32[]{:S(2)}, u32[]{:S(2)}) async-start(bf16[8,128,256]{2,1,0:T(8,128)(2,1)} %bitcast.85), calls=%async_computation.2 | async-start | bytes 1048576 | tf_op jit(solution)/shard_map/all_to_all | solution.py:17
  152.7 13.3 %copy-start.17 = (bf16[176,256]{1,0:T(8,128)(2,1)S(1)}, bf16[176,256]{1,0:T(8,128)(2,1)}, u32[]{:S(2)}) copy-start(bf16[176,256]{1,0:T(8,128)(2,1)} %param.34) | copy-start | bytes 270340
  156.1 20.1 %all-to-all-start.3 = ((bf16[32,4,256]{2,1,0:T(4,128)(2,1)}), bf16[32,4,256]{2,1,0:T(4,128)(2,1)S(1)}, u32[]{:S(2)}, u32[]{:S(2)}) async-start(bf16[32,4,256]{2,1,0:T(4,128)(2,1)} %reshape.388), calls=%async_computation.3 | async-start | bytes 131072 | tf_op jit(solution)/shard_map/all_to_all | solution.py:124
  166.0 14.1 %copy-start.14 = (s32[64]{0:T(128)S(1)}, s32[64]{0:T(128)}, u32[]{:S(2)}) copy-start(s32[64]{0:T(128)} %copy-done.13) | copy-start | bytes 772
  166.0 14.1 %copy-start.16 = (s32[64,1]{0,1:T(1,128)S(1)}, s32[64,1]{0,1:T(1,128)}, u32[]{:S(2)}) copy-start(s32[64,1]{0,1:T(1,128)} %mul.310) | copy-start | bytes 772
  166.0 14.1 %copy-start.11 = (bf16[2048]{0:T(1024)(128)(2,1)S(1)}, bf16[2048]{0:T(1024)(128)(2,1)}, u32[]{:S(2)}) copy-start(bf16[2048]{0:T(1024)(128)(2,1)} %param.31) | copy-start | bytes 12292
  166.0 14.2 %copy-start.15 = (bf16[32,2]{0,1:T(2,128)(2,1)S(1)}, bf16[32,2]{0,1:T(2,128)(2,1)}, u32[]{:S(2)}) copy-start(bf16[32,2]{0,1:T(2,128)(2,1)} %param.36) | copy-start | bytes 388
  166.0 14.3 %copy-start.8 = (f32[32,1,64]{2,0,1:T(8,128)S(1)}, f32[32,1,64]{2,0,1:T(8,128)}, u32[]{:S(2)}) copy-start(f32[32,1,64]{2,0,1:T(8,128)} %copy-done.7) | copy-start | bytes 24580
  166.0 14.3 %copy-start.9 = (f32[32,128]{1,0:T(8,128)S(1)}, f32[32,128]{1,0:T(8,128)}, u32[]{:S(2)}) copy-start(f32[32,128]{1,0:T(8,128)} %get-tuple-element.16) | copy-start | bytes 49156
  176.2 21.6 %all-to-all-start.5 = ((bf16[32,32,256]{2,1,0:T(8,128)(2,1)}), bf16[32,32,256]{2,1,0:T(8,128)(2,1)S(1)}, u32[]{:S(2)}, u32[]{:S(2)}) async-start(bf16[32,32,256]{2,1,0:T(8,128)(2,1)} %bitcast.18), calls=%async_computation.5 | async-start | bytes 1048576 | tf_op jit(solution)/shard_map/all_to_all | solution.py:17
  180.4 2.9 %copy-start.4 = (bf16[32,2048]{1,0:T(8,128)(2,1)S(1)}, bf16[32,2048]{1,0:T(8,128)(2,1)}, u32[]{:S(2)}) copy-start(bf16[32,2048]{1,0:T(8,128)(2,1)} %copy-done.3) | copy-start | bytes 393220
Sparse Core Ops, SparseCore 0:
  82.2 67.4 all-reduce.1
where the time goes:
time: 207 us; the launch traced here: 206 us
  waiting for transfers between devices  105 us (51%)
  starting transfers between devices  40.5 us (20%)
  matrix products  18.1 us (9%)
  local copies, waits for them, and re-layouts  14.9 us (7%)
  between operations  14.5 us (7%)
  other arithmetic  13.4 us (6%)
    psum x1, waiting for transfers between devices, packed_total(): running = lax.psum(flat, axis)  47.7 us
    all_to_all x2, waiting for transfers between devices, copy_for_each(): return lax.all_to_all(copies, axis, split_axis=0, concat_axis=0, tiled=True)  27.9 us
    all_to_all x2, starting transfers between devices, copy_for_each(): return lax.all_to_all(copies, axis, split_axis=0, concat_axis=0, tiled=True)  16 us
    all_to_all x2, waiting for transfers between devices, sent_and_summed(): lax.all_to_all(tiles, axis, split_axis=0, concat_axis=0, tiled=True)  13.4 us
    all_to_all x2, starting transfers between devices, sent_and_summed(): lax.all_to_all(tiles, axis, split_axis=0, concat_axis=0, tiled=True)  9.98 us
    all_to_all x1, starting transfers between devices, padded_experts(): lax.all_to_all(summed.reshape(sources, items, summed.shape[1]), 'ep', spl...  9.82 us
    all_to_all x1, waiting for transfers between devices, padded_experts(): lax.all_to_all(outgoing, 'ep', split_axis=0, concat_axis=0, tiled=True)  8.34 us
    all_to_all x1, waiting for transfers between devices, padded_experts(): lax.all_to_all(summed.reshape(sources, items, summed.shape[1]), 'ep', spl...  7.39 us
  transfers between devices with their start and end apart: 7, of which 6 were waited for; matrix products, arithmetic and copies ran while one was open for 14% of the time, Pallas kernels for 0%

commit v1 on v0

--- a/solution.py
+++ b/solution.py
@@ -41,7 +41,7 @@
 
 def packed_total(arrays, axis):
     flat, at, outs = (jnp.concatenate([a.reshape(-1) for a in arrays]), 0, [])
-    running = lax.psum(flat, axis)
+    running = jnp.sum(lax.all_gather(flat, axis), axis=0)
     for a in arrays:
         outs.append(running[at : at + a.size].reshape(a.shape))
         at += a.size

time: 207 us -> 191 us (0.923)
  waiting for transfers between devices: 105 us -> 33.6 us
  blocking collectives: 0 us -> 49.4 us
  starting transfers between devices: 40.5 us -> 27.6 us
  other arithmetic: 13.4 us -> 25.4 us
  local copies, waits for them, and re-layouts: 14.9 us -> 21.6 us
    all_to_all x0 -> x2, blocking collectives: none -> 49.4 us  [the longest x1 27.9 us: copy_for_each(): return lax.all_to_all(copies, axis, split_axis=0, concat_axis=0, tiled=True)]
    psum x1 -> x0, waiting for transfers between devices: 47.7 us -> none  [packed_total(): running = lax.psum(flat, axis)]
    reduce_sum x0 -> x1, other arithmetic: none -> 14.3 us  [packed_total(): running = jnp.sum(lax.all_gather(flat, axis), axis=0)]
    all_to_all x2 -> x1, waiting for transfers between devices: 27.9 us -> 13.8 us  [copy_for_each(): return lax.all_to_all(copies, axis, split_axis=0, concat_axis=0, tiled=True)]
    all_to_all x2 -> x1, starting transfers between devices: 16 us -> 5.42 us  [copy_for_each(): return lax.all_to_all(copies, axis, split_axis=0, concat_axis=0, tiled=True)]
    all_to_all x1 -> x0, waiting for transfers between devices: 8.34 us -> none  [padded_experts(): lax.all_to_all(outgoing, 'ep', split_axis=0, concat_axis=0, tiled=True)]
    all_gather x0 -> x1, local copies, waits for them, and re-layouts: none -> 7.62 us  [packed_total(): running = jnp.sum(lax.all_gather(flat, axis), axis=0)]
    all_to_all x1, waiting for transfers between devices: 7.39 us -> 0.01 us  [padded_experts(): lax.all_to_all(summed.reshape(sources, items, summed.shape[1]), 'ep', spl...]
  transfers between devices with their start and end apart: 7 -> 5, of which waited for: 6 -> 3; matrix products, arithmetic and copies ran while one was open for 14% -> 24% of each run, Pallas kernels for 0% -> 0%
where the time goes in v1:
time: 191 us; the launch traced here: 189 us
  blocking collectives  49.4 us (26%)
  waiting for transfers between devices  33.6 us (18%)
  starting transfers between devices  27.6 us (14%)
  other arithmetic  25.4 us (13%)
  local copies, waits for them, and re-layouts  21.6 us (11%)
  matrix products  16.5 us (9%)
  between operations  14.5 us (8%)
    all_to_all x1, blocking collectives, copy_for_each(): return lax.all_to_all(copies, axis, split_axis=0, concat_axis=0, tiled=True)  27.9 us
    all_to_all x1, blocking collectives, padded_experts(): lax.all_to_all(outgoing, 'ep', split_axis=0, concat_axis=0, tiled=True)  21.5 us
    all_to_all x2, waiting for transfers between devices, sent_and_summed(): lax.all_to_all(tiles, axis, split_axis=0, concat_axis=0, tiled=True)  19.7 us
    all_to_all x2, starting transfers between devices, sent_and_summed(): lax.all_to_all(tiles, axis, split_axis=0, concat_axis=0, tiled=True)  15 us
    reduce_sum x1, other arithmetic, packed_total(): running = jnp.sum(lax.all_gather(flat, axis), axis=0)  14.3 us
    all_to_all x1, waiting for transfers between devices, copy_for_each(): return lax.all_to_all(copies, axis, split_axis=0, concat_axis=0, tiled=True)  13.8 us
    all_gather x1, local copies, waits for them, and re-layouts, packed_total(): running = jnp.sum(lax.all_gather(flat, axis), axis=0)  7.62 us
    all_to_all x1, starting transfers between devices, padded_experts(): lax.all_to_all(summed.reshape(sources, items, summed.shape[1]), 'ep', spl...  7.24 us
  transfers between devices with their start and end apart: 5, of which 3 were waited for; matrix products, arithmetic and copies ran while one was open for 24% of the time, Pallas kernels for 0%

profile of v1, /device:TPU:24, one launch (start us, length us, event | category | flops | bytes accessed | tf_op | source)
XLA Modules:
  0.0 188.7 jit_solution(4754616117765025900)
XLA Ops:
  7.3 0.8 convert_element_type.128
  8.7 1.0 fusion.25
  10.5 1.4 fusion.18
  11.9 1.4 fusion.20
  13.6 2.0 %fusion.66 = f32[32,1,128]{2,1,0:T(1,128)S(1)} fusion(f32[32,128,1]{1,2,0:T(1,128)S(1)} %bitcast.92, f32[32,1,128,128]{3,2,1,0:T(8,128)} %param.28), kind=kOutput, calls=%fused_computation.103 | convolution fusion | flops 1048576 | bytes 2129920 | tf_op jit(solution)/shard_map/shd,shde->she/dot_general | solution.py:80
  15.6 1.0 fusion.65
  16.8 1.5 convolution_convert_fusion.2
  18.4 1.1 broadcast_in_dim.6
  19.5 5.4 %all-to-all-start = ((bf16[8,32,2048]{2,1,0:T(8,128)(2,1)}), bf16[8,32,2048]{2,1,0:T(8,128)(2,1)S(1)}, u32[]{:S(2)}, u32[]{:S(2)}) async-start(bf16[8,32,2048]{2,1,0:T(8,128)(2,1)} %broadcast_in_dim.6), calls=%async_computation | async-start | bytes 2097152 | tf_op jit(solution)/shard_map/all_to_all | solution.py:23
  24.9 13.8 %all-to-all-done = bf16[8,32,2048]{2,1,0:T(8,128)(2,1)S(1)} async-done(((bf16[8,32,2048]{2,1,0:T(8,128)(2,1)}), bf16[8,32,2048]{2,1,0:T(8,128)(2,1)S(1)}, u32[]{:S(2)}, u32[]{:S(2)}) %all-to-all-start) | async-done | bytes 1048608 | tf_op jit(solution)/shard_map/all_to_all | solution.py:23
  39.8 27.9 %all_to_all.30 = bf16[32,32,256]{2,1,0:T(8,128)(2,1)S(1)} all-to-all(bf16[32,32,256]{2,1,0:T(8,128)(2,1)S(1)} %broadcast_in_dim.8), channel_id=1, replica_groups=mesh['ep'=32,'tp'=8] {'ep'}, dimensions={0} | all-to-all | bytes 1048576 | tf_op jit(solution)/shard_map/all_to_all | solution.py:23
  67.6 1.2 convolution_convert_fusion.4
  71.0 0.9 pad_maximum_fusion
  73.3 21.5 %all_to_all.31 = bf16[32,4,2048]{2,1,0:T(4,128)(2,1)} all-to-all(bf16[32,4,2048]{2,1,0:T(4,128)(2,1)S(1)} %reshape.385), channel_id=1, replica_groups=mesh['ep'=32,'tp'=8] {'ep'}, dimensions={0} | all-to-all | bytes 1048576 | tf_op jit(solution)/shard_map/all_to_all | solution.py:116
  94.9 1.2 reshape.386
  96.0 2.0 %fusion.3 = f32[128,512]{1,0:T(8,128)S(1)} fusion(bf16[128,2048]{1,0:T(8,128)(2,1)S(1)} %reshape.386, bf16[1,2048,512]{2,1,0:T(8,128)(2,1)} %param.37), kind=kOutput, calls=%fused_computation.7 | convolution fusion | flops 268435456 | bytes 2883584 | tf_op jit(solution)/shard_map/dot_general | solution.py:96
  98.1 2.5 %convolution_convert_fusion = bf16[128,2048]{1,0:T(8,128)(2,1)S(1)} fusion(bf16[1,512,2048]{2,1,0:T(8,128)(2,1)S(1)} %copy-done, bf16[128,2048]{1,0:T(8,128)(2,1)S(1)} %reshape.386, bf16[1,2048,512]{2,1,0:T(8,128)(2,1)} %param.38, f32[128,512]{1,0:T(8,128)S(1)} %fusion.3), kind=kOutput, calls=%fused_computation.1 | convolution fusion | flops 537526272 | bytes 5505024 | tf_op jit(solution)/shard_map/dot_general | solution.py:122
  100.6 0.8 copy.46
  101.4 5.5 %all-to-all-start.2 = ((bf16[8,128,256]{2,1,0:T(8,128)(2,1)}), bf16[8,128,256]{2,1,0:T(8,128)(2,1)S(1)}, u32[]{:S(2)}, u32[]{:S(2)}) async-start(bf16[8,128,256]{2,1,0:T(8,128)(2,1)} %bitcast.85), calls=%async_computation.2 | async-start | bytes 1048576 | tf_op jit(solution)/shard_map/all_to_all | solution.py:17
  107.6 7.5 %all-to-all-done.2 = bf16[8,128,256]{2,1,0:T(8,128)(2,1)S(1)} async-done(((bf16[8,128,256]{2,1,0:T(8,128)(2,1)}), bf16[8,128,256]{2,1,0:T(8,128)(2,1)S(1)}, u32[]{:S(2)}, u32[]{:S(2)}) %all-to-all-start.2) | async-done | bytes 524320 | tf_op jit(solution)/shard_map/all_to_all | solution.py:17
  115.8 7.2 %all-to-all-start.3 = ((bf16[32,4,256]{2,1,0:T(4,128)(2,1)}), bf16[32,4,256]{2,1,0:T(4,128)(2,1)}, u32[]{:S(2)}, u32[]{:S(2)}) async-start(bf16[32,4,256]{2,1,0:T(4,128)(2,1)} %reshape.388), calls=%async_computation.3 | async-start | bytes 131072 | tf_op jit(solution)/shard_map/all_to_all | solution.py:124
  123.1 7.6 %reshape.412 = bf16[8,360448]{1,0:T(8,128)(2,1)} reshape(bf16[2883584]{0:T(1024)(128)(2,1)} %all-gather.3.cloned.1.call-done) | data formatting | bytes 11534336 | tf_op jit(solution)/shard_map/all_gather | solution.py:44
  130.7 14.3 %reduce_sum.117 = bf16[360448]{0:T(1024)(128)(2,1)S(1)} reduce(bf16[8,360448]{1,0:T(8,128)(2,1)} %reshape.412, bf16[]{:T(256)} %constant.62.clone.1), dimensions={0}, to_apply=%region_10.11 | reduce | flops 2523136 | bytes 6488066 | tf_op jit(solution)/shard_map/reduce_sum | solution.py:44
  145.0 1.0 slice_convert_fusion.1
  146.0 2.9 %reshape.401 = f32[1024,176]{1,0:T(8,128)} reshape(f32[180224]{0:T(1024)} %get-tuple-element.8) | data formatting | bytes 1441792 | tf_op jit(solution)/shard_map/convert_element_type | solution.py:202
  148.9 1.7 reshape.402
  150.6 2.8 %convolution_convert_fusion.3 = bf16[1024,256]{1,0:T(8,128)(2,1)} fusion(bf16[176,256]{1,0:T(8,128)(2,1)S(1)} %copy-done.19, f32[1024,176]{1,0:T(8,128)} %reshape.402, f32[1024,176]{1,0:T(8,128)} %reshape.401), kind=kOutput, calls=%fused_computation.13 | convolution fusion | flops 93618176 | bytes 2056192 | tf_op jit(solution)/shard_map/dot_general | solution.py:210
  153.4 9.5 %all-to-all-start.5 = ((bf16[32,32,256]{2,1,0:T(8,128)(2,1)}), bf16[32,32,256]{2,1,0:T(8,128)(2,1)S(1)}, u32[]{:S(2)}, u32[]{:S(2)}) async-start(bf16[32,32,256]{2,1,0:T(8,128)(2,1)} %bitcast.18), calls=%async_computation.5 | async-start | bytes 1048576 | tf_op jit(solution)/shard_map/all_to_all | solution.py:17
  163.2 2.9 %multiply_add_fusion = f32[32,1,128,128]{3,2,1,0:T(8,128)} fusion(f32[32,1,128,128]{3,2,1,0:T(8,128)} %param.28, f32[32,128]{1,0:T(8,128)S(1)} %copy-done.10, f32[32,128]{1,0:T(8,128)S(1)} %maximum_multiply_fusion.1, f32[]{:T(128)S(6)} %sub.37), kind=kLoop, calls=%fused_computation.11 | loop fusion | flops 1572864 | bytes 4227076 | tf_op jit(solution)/shard_map/add | solution.py:83
  166.3 0.9 reshape.389
  168.1 12.2 %all-to-all-done.5 = bf16[32,32,256]{2,1,0:T(8,128)(2,1)S(1)} async-done(((bf16[32,32,256]{2,1,0:T(8,128)(2,1)}), bf16[32,32,256]{2,1,0:T(8,128)(2,1)S(1)}, u32[]{:S(2)}, u32[]{:S(2)}) %all-to-all-start.5) | async-done | bytes 524320 | tf_op jit(solution)/shard_map/all_to_all | solution.py:17
  180.4 1.4 add_convert_fusion
  (90 shorter events, 9.2 us)
Async XLA Ops:
  7.2 90.9 %copy-start = (bf16[1,512,2048]{2,1,0:T(8,128)(2,1)S(1)}, bf16[1,512,2048]{2,1,0:T(8,128)(2,1)}, u32[]{:S(2)}) copy-start(bf16[1,512,2048]{2,1,0:T(8,128)(2,1)} %param.39) | copy-start | bytes 6291460
  7.2 8.4 %copy-start.1 = (bf16[32,2048]{1,0:T(8,128)(2,1)S(1)}, bf16[32,2048]{1,0:T(8,128)(2,1)}, u32[]{:S(2)}) copy-start(bf16[32,2048]{1,0:T(8,128)(2,1)} %param.20) | copy-start | bytes 393220
  7.2 8.4 %copy-start.5 = (bf16[2048,128]{1,0:T(8,128)(2,1)S(1)}, bf16[2048,128]{1,0:T(8,128)(2,1)}, u32[]{:S(2)}) copy-start(bf16[2048,128]{1,0:T(8,128)(2,1)} %param.24) | copy-start | bytes 1572868
  10.5 6.3 %copy-start.6 = (bf16[128,2048]{1,0:T(8,128)(2,1)S(1)}, bf16[128,2048]{1,0:T(8,128)(2,1)}, u32[]{:S(2)}) copy-start(bf16[128,2048]{1,0:T(8,128)(2,1)} %param.27) | copy-start | bytes 1572868
  13.4 4.9 %copy-start.7 = (f32[32,1,64]{2,0,1:T(8,128)}, f32[32,1,64]{2,0,1:T(8,128)S(1)}, u32[]{:S(2)}) copy-start(f32[32,1,64]{2,0,1:T(8,128)S(1)} %get-tuple-element.15) | copy-start | bytes 24580
  16.8 8.1 %copy-start.11 = (bf16[2048]{0:T(1024)(128)(2,1)S(1)}, bf16[2048]{0:T(1024)(128)(2,1)}, u32[]{:S(2)}) copy-start(bf16[2048]{0:T(1024)(128)(2,1)} %param.30) | copy-start | bytes 12292
  19.5 19.3 %all-to-all-start = ((bf16[8,32,2048]{2,1,0:T(8,128)(2,1)}), bf16[8,32,2048]{2,1,0:T(8,128)(2,1)S(1)}, u32[]{:S(2)}, u32[]{:S(2)}) async-start(bf16[8,32,2048]{2,1,0:T(8,128)(2,1)} %broadcast_in_dim.6), calls=%async_computation | async-start | bytes 2097152 | tf_op jit(solution)/shard_map/all_to_all | solution.py:23
  24.9 98.2 %all-gather.3.cloned.1.call-start = ((), (), s32[]{:S(2)}) async-start(), calls=%async_computation.6 | async-start | bytes 6488064 | tf_op jit(solution)/shard_map/all_gather | solution.py:44
  38.9 30.0 %copy-start.9 = (bf16[256,176]{0,1:T(8,128)(2,1)S(1)}, bf16[256,176]{0,1:T(8,128)(2,1)}, u32[]{:S(2)}) copy-start(bf16[256,176]{0,1:T(8,128)(2,1)} %param.32) | copy-start | bytes 270340
  39.0 0.7 copy-start.2
  39.1 33.4 %copy-start.3 = (bf16[32,2048]{1,0:T(8,128)(2,1)}, bf16[32,2048]{1,0:T(8,128)(2,1)S(1)}, u32[]{:S(2)}) copy-start(bf16[32,2048]{1,0:T(8,128)(2,1)S(1)} %multiply_convert_fusion.2) | copy-start | bytes 393220
  70.1 1.9 copy-start.13
  72.5 23.5 %copy-start.15 = (s32[64]{0:T(128)}, s32[64]{0:T(128)S(1)}, u32[]{:S(2)}) copy-start(s32[64]{0:T(128)S(1)} %select_reduce_fusion) | copy-start | bytes 772
  100.6 6.3 %copy-start.14 = (s32[32,2]{0,1:T(2,128)S(1)}, s32[32,2]{0,1:T(2,128)}, u32[]{:S(2)}) copy-start(s32[32,2]{0,1:T(2,128)} %param.35) | copy-start | bytes 772
  101.4 13.7 %all-to-all-start.2 = ((bf16[8,128,256]{2,1,0:T(8,128)(2,1)}), bf16[8,128,256]{2,1,0:T(8,128)(2,1)S(1)}, u32[]{:S(2)}, u32[]{:S(2)}) async-start(bf16[8,128,256]{2,1,0:T(8,128)(2,1)} %bitcast.85), calls=%async_computation.2 | async-start | bytes 1048576 | tf_op jit(solution)/shard_map/all_to_all | solution.py:17
  115.8 37.6 %all-to-all-start.3 = ((bf16[32,4,256]{2,1,0:T(4,128)(2,1)}), bf16[32,4,256]{2,1,0:T(4,128)(2,1)}, u32[]{:S(2)}, u32[]{:S(2)}) async-start(bf16[32,4,256]{2,1,0:T(4,128)(2,1)} %reshape.388), calls=%async_computation.3 | async-start | bytes 131072 | tf_op jit(solution)/shard_map/all_to_all | solution.py:124
  146.0 4.6 %copy-start.19 = (bf16[176,256]{1,0:T(8,128)(2,1)S(1)}, bf16[176,256]{1,0:T(8,128)(2,1)}, u32[]{:S(2)}) copy-start(bf16[176,256]{1,0:T(8,128)(2,1)} %param.34) | copy-start | bytes 270340
  150.6 12.4 %copy-start.16 = (s32[64]{0:T(128)S(1)}, s32[64]{0:T(128)}, u32[]{:S(2)}) copy-start(s32[64]{0:T(128)} %copy-done.15) | copy-start | bytes 772
  150.6 12.4 %copy-start.18 = (s32[64,1]{0,1:T(1,128)S(1)}, s32[64,1]{0,1:T(1,128)}, u32[]{:S(2)}) copy-start(s32[64,1]{0,1:T(1,128)} %mul.310) | copy-start | bytes 772
  150.6 12.4 %copy-start.12 = (bf16[2048]{0:T(1024)(128)(2,1)S(1)}, bf16[2048]{0:T(1024)(128)(2,1)}, u32[]{:S(2)}) copy-start(bf16[2048]{0:T(1024)(128)(2,1)} %param.31) | copy-start | bytes 12292
  150.6 12.4 %copy-start.17 = (bf16[32,2]{0,1:T(2,128)(2,1)S(1)}, bf16[32,2]{0,1:T(2,128)(2,1)}, u32[]{:S(2)}) copy-start(bf16[32,2]{0,1:T(2,128)(2,1)} %param.36) | copy-start | bytes 388
  150.6 12.5 %copy-start.8 = (f32[32,1,64]{2,0,1:T(8,128)S(1)}, f32[32,1,64]{2,0,1:T(8,128)}, u32[]{:S(2)}) copy-start(f32[32,1,64]{2,0,1:T(8,128)} %copy-done.7) | copy-start | bytes 24580
  150.6 12.6 %copy-start.10 = (f32[32,128]{1,0:T(8,128)S(1)}, f32[32,128]{1,0:T(8,128)}, u32[]{:S(2)}) copy-start(f32[32,128]{1,0:T(8,128)} %get-tuple-element.16) | copy-start | bytes 49156
  153.4 26.9 %all-to-all-start.5 = ((bf16[32,32,256]{2,1,0:T(8,128)(2,1)}), bf16[32,32,256]{2,1,0:T(8,128)(2,1)S(1)}, u32[]{:S(2)}, u32[]{:S(2)}) async-start(bf16[32,32,256]{2,1,0:T(8,128)(2,1)} %bitcast.18), calls=%async_computation.5 | async-start | bytes 1048576 | tf_op jit(solution)/shard_map/all_to_all | solution.py:17
  163.2 2.9 %copy-start.4 = (bf16[32,2048]{1,0:T(8,128)(2,1)S(1)}, bf16[32,2048]{1,0:T(8,128)(2,1)}, u32[]{:S(2)}) copy-start(bf16[32,2048]{1,0:T(8,128)(2,1)} %copy-done.3) | copy-start | bytes 393220
Sparse Core Ops, SparseCore 0:
  72.1 35.1 all-gather.2
